TPU v7x, 32 devices: a whole 2x2x4 slice. The times are simulated.
32 devices in a mesh: sp: 8 (over z, y), tp: 4 (over x, core).
Axes of the slice: x: 2, y: 2, z: 4, core: 2. Of those that a mesh axis runs over, the one named last changes fastest.
Arguments:
- tokens: bfloat16 [2048, 4096], P(('sp', 'tp')), may hold values from -6 to 6
- norm_gain: float32 [4096], replicated, may hold values from 0.1 to 1.9
- w_query: bfloat16 [4096, 1024], P(None, 'tp'), may hold values from -0.25 to 0.25
- w_key: bfloat16 [4096, 512], P(None, 'tp'), may hold values from -0.09375 to 0.09375
- w_value: bfloat16 [4096, 512], P(None, 'tp'), may hold values from -0.09375 to 0.09375
- score_shift: float32 [8], P('tp'), may hold values from -15 to -8
- w_conv_b: bfloat16 [4096, 1024], P(None, 'tp'), may hold values from -0.09375 to 0.09375
- w_conv_c: bfloat16 [4096, 1024], P(None, 'tp'), may hold values from -0.09375 to 0.09375
- w_conv_u: bfloat16 [4096, 1024], P(None, 'tp'), may hold values from -0.09375 to 0.09375
- conv_kernel: float32 [3, 1024], P(None, 'tp'), may hold values from -3.5 to 3.5
- w_out_att: bfloat16 [4096, 1024], P('sp', 'tp'), may hold values from -0.75 to 0.75
- w_out_conv: bfloat16 [4096, 1024], P('sp', 'tp'), may hold values from -0.1875 to 0.1875
Outputs:
- mixed: bfloat16 [2048, 4096], P(('sp', 'tp'))
- log_weight: float32 [2048, 8], P('sp', 'tp')
All inputs are finite; a program needn't handle non-finite values.
Results may differ from a plain program's by a relative error of at most 0.017.
Values may be sent and summed in bfloat16 or wider, within the bound.
A program may use at most 128 MiB of HBM per device.

v0:
```python
import jax
import jax.numpy as jnp
from jax import lax
from jax.sharding import PartitionSpec as P

HEAD_DIM = 128
CONV_K = 3
KEY_BLOCK = 1024


def swapped(block, axis, stride):
    count = lax.axis_size(axis)
    route = []
    for low in range(count):
        high = low | 1 << stride
        if high != low and high < count:
            route += [(low, high), (high, low)]
    return lax.ppermute(block, axis, route)


def shifted(value, axis, steps):
    count = lax.axis_size(axis)
    leading, last = (max(0, -steps), min(count, count - steps))
    return lax.ppermute(value, axis, [(source, source + steps) for source in range(leading, last)])


def normalize(tokens, norm_gain):
    widened = tokens.astype(jnp.float32)
    inverse = lax.rsqrt(jnp.mean(widened * widened, axis=-1, keepdims=True) + 1e-06)
    return (widened * inverse * norm_gain).astype(jnp.bfloat16)


def block_terms(grouped_q, key_block, value_block, shifts, query_pos, key_first):
    scores = jnp.einsum("qhgd,khd->qhgk", grouped_q, key_block, preferred_element_type=jnp.float32)
    scores = scores * HEAD_DIM ** (-0.5) + shifts[None, :, :, None]
    key_pos = key_first + jnp.arange(KEY_BLOCK, dtype=jnp.int32)
    causal = key_pos[None, None, None, :] < query_pos[:, None, None, None]
    soft = jnp.where(causal, jax.nn.softplus(scores), 0.0)
    after_sum = lax.cumsum(soft, axis=3, reverse=True) - soft
    relative = jnp.where(causal, jnp.exp(jax.nn.log_sigmoid(scores) - after_sum), 0.0).astype(
        jnp.bfloat16
    )
    partial_value = jnp.einsum(
        "qhgk,khd->qhgd", relative, value_block, preferred_element_type=jnp.float32
    )
    return (partial_value, jnp.sum(soft, axis=3))


def attend(grouped_q, query_pos, key_whole, value_whole, shifts):
    row_count, kv_local, grouping, head_size = grouped_q.shape
    last_block = jnp.max(query_pos) // KEY_BLOCK

    def visit(step, carry):
        accum, suffix = carry
        block_no = last_block - step
        key_first = block_no * KEY_BLOCK
        key_block = lax.dynamic_slice_in_dim(key_whole, key_first, KEY_BLOCK, 0).reshape(
            KEY_BLOCK, kv_local, head_size
        )
        value_block = lax.dynamic_slice_in_dim(value_whole, key_first, KEY_BLOCK, 0).reshape(
            KEY_BLOCK, kv_local, head_size
        )
        partial_value, total = block_terms(
            grouped_q, key_block, value_block, shifts, query_pos, key_first
        )
        accum = accum + jnp.exp(-suffix)[..., None] * partial_value
        return (accum, suffix + total)

    start = (
        jnp.zeros((row_count, kv_local, grouping, head_size), jnp.float32),
        jnp.zeros((row_count, kv_local, grouping), jnp.float32),
    )
    accum, suffix = lax.fori_loop(0, last_block + 1, visit, start)
    return (
        accum.reshape(row_count, kv_local * grouping * head_size),
        suffix.reshape(row_count, kv_local * grouping),
    )


def mirror_queries(payload):
    for bit in range(lax.axis_size("sp").bit_length() - 1):
        payload = swapped(payload, "sp", bit)
    return payload


def mirror_results(payload):
    for bit in range(lax.axis_size("sp").bit_length() - 1):
        payload = (
            swapped(payload[0].astype(jnp.bfloat16), "sp", bit).astype(jnp.float32),
            swapped(payload[1].astype(jnp.bfloat16), "sp", bit).astype(jnp.float32),
        )
    return payload


def local(
    tokens,
    norm_gain,
    w_query,
    w_key,
    w_value,
    score_shift,
    w_conv_b,
    w_conv_c,
    w_conv_u,
    conv_kernel,
    w_out_att,
    w_out_conv,
):
    weights = (w_query, w_key, w_value, w_conv_b, w_conv_c, w_conv_u)

    def project(rows_in):
        normed = normalize(rows_in, norm_gain)
        return jnp.concatenate(
            [
                jnp.dot(normed, weight, preferred_element_type=jnp.float32).astype(jnp.bfloat16)
                for weight in weights
            ],
            axis=1,
        )

    projected = project(lax.all_gather(tokens, "tp", axis=0, tiled=True))
    widths = [weight.shape[1] for weight in weights]
    edges = [0]
    for width in widths:
        edges.append(edges[-1] + width)
    queries, keys, values, gate_b, gate_c, inputs_u = [
        projected[:, edges[pos] : edges[pos + 1]] for pos in range(6)
    ]
    tok_count = projected.shape[0]
    conv_local = gate_b.shape[1]
    products = (gate_c.astype(jnp.float32) * inputs_u.astype(jnp.float32)).astype(jnp.bfloat16)
    previous = shifted(products[tok_count - (CONV_K - 1) :], "sp", 1)
    key_whole, value_whole = (
        lax.all_gather(keys, "sp", axis=0, tiled=True),
        lax.all_gather(values, "sp", axis=0, tiled=True),
    )
    local_heads = queries.shape[1] // HEAD_DIM
    kv_local = keys.shape[1] // HEAD_DIM
    grouping = local_heads // kv_local
    shifts = score_shift.reshape(kv_local, grouping)
    sp_count = lax.axis_size("sp")
    sp_index = lax.axis_index("sp")
    half = tok_count // 2
    own_q = queries[:half].reshape(half, kv_local, grouping, HEAD_DIM)
    own_pos = sp_index * tok_count + jnp.arange(half, dtype=jnp.int32)
    own_att, own_sums = attend(own_q, own_pos, key_whole, value_whole, shifts)
    other_q = mirror_queries(queries[half:]).reshape(tok_count - half, kv_local, grouping, HEAD_DIM)
    other_pos = (
        (sp_count - 1 - sp_index) * tok_count + half + jnp.arange(tok_count - half, dtype=jnp.int32)
    )
    other_att, other_sums = attend(other_q, other_pos, key_whole, value_whole, shifts)
    back_att, back_sums = mirror_results((other_att, other_sums))
    attended_f = jnp.concatenate([own_att, back_att], axis=0)
    sums_all = jnp.concatenate([own_sums, back_sums], axis=0)
    attended = attended_f.astype(jnp.bfloat16)
    log_weight = jnp.log(jnp.maximum(-jnp.expm1(-sums_all), 0.05))
    extended = jnp.concatenate([previous, products], axis=0)
    summed = jnp.zeros((tok_count, conv_local), jnp.float32)
    for tap in range(CONV_K):
        summed = summed + conv_kernel[tap][None, :] * extended[tap : tap + tok_count].astype(
            jnp.float32
        )
    convolved = (gate_b.astype(jnp.float32) * summed).astype(jnp.bfloat16)
    contract = (((1,), (1,)), ((), ()))
    pieces = lax.all_gather((w_out_att, w_out_conv), "sp", axis=0, tiled=True)
    result = lax.dot_general(attended, pieces[0], contract, preferred_element_type=jnp.float32)
    share = result + lax.dot_general(
        convolved, pieces[1], contract, preferred_element_type=jnp.float32
    )
    rounded = share.astype(jnp.bfloat16).astype(jnp.float32)
    mixed = lax.psum_scatter(rounded.astype(jnp.bfloat16), "tp", scatter_dimension=0, tiled=True)
    return (mixed, log_weight)


def solution(mesh):
    return jax.shard_map(
        local,
        mesh=mesh,
        in_specs=(
            P(("sp", "tp"), None),
            P(),
            P(None, "tp"),
            P(None, "tp"),
            P(None, "tp"),
            P("tp"),
            P(None, "tp"),
            P(None, "tp"),
            P(None, "tp"),
            P(None, "tp"),
            P("sp", "tp"),
            P("sp", "tp"),
        ),
        out_specs=(P(("sp", "tp"), None), P("sp", "tp")),
        check_vma=False,
    )
```

profile of v0, /device:TPU:0, one launch (start us, length us, event | category | flops | bytes accessed | tf_op | source)
XLA Modules:
  0.0 195.4 jit_solution(12022105615553564514)
XLA Ops:
  7.2 0.7 all-gather.4.cloned.1.call-update
  8.0 0.7 all-gather.8.cloned.1.call-update
  8.7 0.7 all-gather.6.cloned.1.call-update
  9.5 0.6 add_reduce_fusion
  12.0 0.7 add_reduce_fusion.1
  15.9 0.8 fusion.88
  16.7 18.2 %all-gather.4.cloned.1.call-done = bf16[256,4096]{1,0:T(8,128)(2,1)} async-done(((bf16[64,4096]{1,0:T(8,128)(2,1)}), bf16[256,4096]{1,0:T(8,128)(2,1)}) %all-gather.4.cloned.1.call-update) | async-done | bytes 2097168 | tf_op jit(solution)/shard_map/all_gather | solution.py:121
  34.9 2.2 %fusion.53 = f32[256]{0:T(256)S(1)} fusion(bf16[256,4096]{1,0:T(8,128)(2,1)} %all-gather.4.cloned.1.call-done), kind=kLoop, calls=%fused_computation.78 | loop fusion | flops 3145472 | bytes 2098176 | tf_op jit(solution)/shard_map/reduce_sum | solution.py:29
  37.1 0.6 fusion.55
  37.8 0.6 copy-done.9
  38.4 0.7 convolution_convert_fusion.5
  39.1 1.6 copy-done.7
  40.7 1.0 convolution_convert_fusion.3
  41.7 1.5 collective-permute-start
  43.3 1.4 fusion.59
  44.7 0.7 convolution_convert_fusion.4
  45.4 0.7 collective-permute-done
  46.0 1.5 collective-permute-start.1
  47.5 33.3 %all_gather.16 = bf16[2048,128]{1,0:T(8,128)(2,1)S(1)} all-gather(bf16[256,128]{1,0:T(8,128)(2,1)S(1)} %convolution_convert_fusion.5), channel_id=1, replica_groups=mesh['sp'=8,'tp'=4] {'sp'}, dimensions={0}, use_global_device_ids=true | all-gather | bytes 589824 | tf_op jit(solution)/shard_map/all_gather | solution.py:135
  80.9 32.5 %all_gather.17 = bf16[2048,128]{1,0:T(8,128)(2,1)S(1)} all-gather(bf16[256,128]{1,0:T(8,128)(2,1)S(1)} %convolution_convert_fusion.4), channel_id=1, replica_groups=mesh['sp'=8,'tp'=4] {'sp'}, dimensions={0}, use_global_device_ids=true | all-gather | bytes 589824 | tf_op jit(solution)/shard_map/all_gather | solution.py:134
  113.3 1.0 copy.20
  114.5 15.4 %while.27 = (s32[]{:T(128)}, f32[128,1,2,128]{0,3,2,1:T(8,128)S(1)}, f32[128,1,2]{0,2,1:T(2,128)S(1)}, s32[]{:T(128)}, s32[]{:T(128)}, /*index=5*/bf16[2048,128]...) while((s32[]{:T(128)}, ...), condition=%wide.region_12.13_spmd.clone, body=%wide.region_8.12_spmd.clone.sunk | while | flops 175588480 | bytes 23864196 | solution.py:73
  114.8 1.9 fusion.127
  116.6 2.5 %fusion.128 = f32[128,1,2,8,128]{0,3,2,1,4:T(8,128)S(1)} fusion(f32[128,1,2,8,128]{0,4,3,2,1:T(8,128)S(1)} %bitcast.178), kind=kOutput, calls=%fused_computation.56.clone.1 | output fusion | flops 33292288 | bytes 2097152 | tf_op jit(solution)/shard_map/reduce-window.2
  119.7 0.8 copy-done.2
  120.4 1.5 fusion.129
  122.5 1.8 fusion.127
  124.3 2.5 %fusion.128 = f32[128,1,2,8,128]{0,3,2,1,4:T(8,128)S(1)} fusion(f32[128,1,2,8,128]{0,4,3,2,1:T(8,128)S(1)} %bitcast.178), kind=kOutput, calls=%fused_computation.56.clone.1 | output fusion | flops 33292288 | bytes 2097152 | tf_op jit(solution)/shard_map/reduce-window.2
  127.3 0.8 copy-done.2
  128.1 1.5 fusion.129
  130.0 2.9 %fusion.58 = bf16[256,256]{1,0:T(8,128)(2,1)S(1)} fusion(f32[256,256]{1,0:T(8,128)} %fusion.59, bf16[256,4096]{1,0:T(8,128)(2,1)} %copy-done.1, bf16[4096,256]{1,0:T(8,128)(2,1)} %param.24), kind=kOutput, calls=%fused_computation.84 | convolution fusion | flops 537133056 | bytes 4587520 | tf_op jit(solution)/shard_map/dot_general | solution.py:115
  133.1 3.9 %collective-permute-start.6 = (bf16[2,256]{1,0:T(2,128)(2,1)S(1)}, bf16[2,256]{1,0:T(2,128)(2,1)S(1)}, u32[]{:S(2)}, u32[]{:S(2)}) collective-permute-start(bf16[2,256]{1,0:T(2,128)(2,1)S(1)} %slice.54), channel_id=1, source_target_pairs={{0,4},{4,8},{8,12},{12,16},{16,20},{20,24},{24,28},{1,5},{5,9},{9,... | collective-permute-start | bytes 3080 | tf_op jit(solution)/shard_map/ppermute | solution.py:24
  137.1 7.9 %while.26 = (s32[]{:T(128)}, f32[128,1,2,128]{0,3,2,1:T(8,128)S(1)}, f32[128,1,2]{0,2,1:T(2,128)S(1)}, s32[]{:T(128)}, s32[]{:T(128)}, /*index=5*/bf16[2048,128]...) while((s32[]{:T(128)}, ...), condition=%wide.region_6.7_spmd.clone, body=%wide.region_2.6_spmd.clone.sunk | while | flops 175588480 | bytes 23864196 | solution.py:73
  137.6 1.8 fusion.120
  139.4 2.5 %fusion.121 = f32[128,1,2,8,128]{0,3,2,1,4:T(8,128)S(1)} fusion(f32[128,1,2,8,128]{0,4,3,2,1:T(8,128)S(1)} %bitcast.179), kind=kOutput, calls=%fused_computation.20.clone.1 | output fusion | flops 33292288 | bytes 2097152 | tf_op jit(solution)/shard_map/reduce-window
  142.5 0.8 copy-done.3
  143.2 1.5 fusion.122
  145.0 2.2 %collective-permute-start.5 = (bf16[128,256]{0,1:T(8,128)(2,1)}, bf16[128,256]{0,1:T(8,128)(2,1)S(1)}, u32[]{:S(2)}, u32[]{:S(2)}) collective-permute-start(bf16[128,256]{0,1:T(8,128)(2,1)} %collective-permute-done.4), channel_id=1, source_target_pairs={{0,16},{16,0},{4,20},{20,4},{8,24},{24,8},{12,28},{28,12},{1,17},{... | collective-permute-start | bytes 196616 | tf_op jit(solution)/shard_map/ppermute | solution.py:18
  147.2 6.6 %fusion.63 = f32[256,4096]{1,0:T(8,128)} fusion(bf16[4096,256]{1,0:T(8,128)(2,1)} %all-gather.8.cloned.1.call-done, bf16[256,4096]{1,0:T(8,128)(2,1)} %copy-done.1, bf16[4096,256]{1,0:T(8,128)(2,1)S(1)} %copy-done, bf16[256,256]{1,0:T(8,128)(2,1)} %copy-done.11, bf16[2,256]{1,0:T(2,128)(2,1)S(1)} %collective-permute-done.6, f32[256]{0:T(256)S(1)} %bitcast.186, ...), kind=kOutput, calls=%fused_computation.92 | convolution fusion | flops 1074921472 | bytes 10620928 | tf_op jit(solution)/shard_map/dot_general | solution.py:167
  153.9 5.0 %fusion.52 = bf16[256,4096]{1,0:T(8,128)(2,1)} fusion(f32[256,4096]{1,0:T(8,128)} %fusion.63, bf16[4096,256]{1,0:T(8,128)(2,1)} %all-gather.6.cloned.1.call-done, bf16[128,256]{0,1:T(8,128)(2,1)S(1)} %collective-permute-done.5, bf16[128,256]{0,1:T(8,128)(2,1)S(1)} %bitcast.180), kind=kOutput, calls=%fused_computation.77 | convolution fusion | flops 539230208 | bytes 8519680 | tf_op jit(solution)/shard_map/dot_general | solution.py:166
  158.9 1.3 collective-permute-start.7
  160.1 2.4 %collective-permute-done.7 = bf16[128,2]{0,1:T(2,128)(2,1)S(1)} collective-permute-done((bf16[128,2]{0,1:T(2,128)(2,1)S(1)}, bf16[128,2]{0,1:T(2,128)(2,1)S(1)}, u32[]{:S(2)}, u32[]{:S(2)}) %collective-permute-start.7) | collective-permute-done | bytes 544 | tf_op jit(solution)/shard_map/ppermute | solution.py:18
  162.5 1.2 collective-permute-start.8
  163.7 2.4 %collective-permute-done.8 = bf16[128,2]{0,1:T(2,128)(2,1)S(1)} collective-permute-done((bf16[128,2]{0,1:T(2,128)(2,1)S(1)}, bf16[128,2]{0,1:T(2,128)(2,1)S(1)}, u32[]{:S(2)}, u32[]{:S(2)}) %collective-permute-start.8) | collective-permute-done | bytes 544 | tf_op jit(solution)/shard_map/ppermute | solution.py:18
  166.1 0.8 collective-permute-start.9
  166.9 3.6 %collective-permute-done.9 = bf16[128,2]{0,1:T(2,128)(2,1)S(1)} collective-permute-done((bf16[128,2]{0,1:T(2,128)(2,1)S(1)}, bf16[128,2]{0,1:T(2,128)(2,1)S(1)}, u32[]{:S(2)}, u32[]{:S(2)}) %collective-permute-start.9) | collective-permute-done | bytes 544 | tf_op jit(solution)/shard_map/ppermute | solution.py:18
  170.5 0.6 fusion.84
  171.1 17.7 %reduce-scatter.2.cloned.1.call-done = bf16[64,4096]{1,0:T(8,128)(2,1)} async-done(((bf16[256,4096]{1,0:T(8,128)(2,1)}), bf16[64,4096]{1,0:T(8,128)(2,1)}) %reduce-scatter.2.cloned.1.call-update) | async-done | bytes 524304 | tf_op jit(solution)/shard_map/reduce_scatter | solution.py:171
  (110 shorter events, 3.5 us)
Async XLA Ops:
  7.2 140.1 %copy-start = (bf16[4096,256]{1,0:T(8,128)(2,1)S(1)}, bf16[4096,256]{1,0:T(8,128)(2,1)}, u32[]{:S(2)}) copy-start(bf16[4096,256]{1,0:T(8,128)(2,1)} %param.22) | copy-start | bytes 6291460
  7.2 29.9 %copy-start.20 = (f32[4096]{0:T(1024)S(1)}, f32[4096]{0:T(1024)}, u32[]{:S(2)}) copy-start(f32[4096]{0:T(1024)} %param.17) | copy-start | bytes 49156
  7.2 27.7 %all-gather.4.cloned.1.call-start = ((), (), s32[]{:S(2)}) async-start(), calls=%async_computation.1 | async-start | bytes 2621440 | tf_op jit(solution)/shard_map/all_gather | solution.py:121
  7.9 139.3 %all-gather.8.cloned.1.call-start = ((), (), s32[]{:S(2)}) async-start(), calls=%async_computation.3 | async-start | bytes 2359296 | tf_op jit(solution)/shard_map/all_gather | solution.py:165
  8.7 145.2 %all-gather.6.cloned.1.call-start = ((), (), s32[]{:S(2)}) async-start(), calls=%async_computation.2 | async-start | bytes 2359296 | tf_op jit(solution)/shard_map/all_gather | solution.py:165
  9.4 179.5 %reduce-scatter.2.cloned.1.call-start = ((), (), s32[]{:S(2)}) async-start(), calls=%async_computation.4 | async-start | bytes 2621440 | tf_op jit(solution)/shard_map/reduce_scatter | solution.py:171
  34.9 2.3 %copy-start.6 = (bf16[256,4096]{1,0:T(8,128)(2,1)S(1)}, bf16[256,4096]{1,0:T(8,128)(2,1)}, u32[]{:S(2)}) copy-start(bf16[256,4096]{1,0:T(8,128)(2,1)} %all-gather.4.cloned.1.call-done) | copy-start | bytes 6291460
  37.1 1.2 copy-start.9
  38.4 6.3 %copy-start.1 = (bf16[256,4096]{1,0:T(8,128)(2,1)}, bf16[256,4096]{1,0:T(8,128)(2,1)S(1)}, u32[]{:S(2)}) copy-start(bf16[256,4096]{1,0:T(8,128)(2,1)S(1)} %fusion.55) | copy-start | bytes 6291460
  38.4 2.3 %copy-start.7 = (bf16[4096,256]{1,0:T(8,128)(2,1)S(1)}, bf16[4096,256]{1,0:T(8,128)(2,1)}, u32[]{:S(2)}) copy-start(bf16[4096,256]{1,0:T(8,128)(2,1)} %param.18) | copy-start | bytes 6291460
  40.7 2.5 %copy-start.8 = (bf16[4096,256]{1,0:T(8,128)(2,1)S(1)}, bf16[4096,256]{1,0:T(8,128)(2,1)}, u32[]{:S(2)}) copy-start(bf16[4096,256]{1,0:T(8,128)(2,1)} %param.23) | copy-start | bytes 6291460
  41.7 3.0 %copy-start.10 = (bf16[4096,128]{1,0:T(8,128)(2,1)S(1)}, bf16[4096,128]{1,0:T(8,128)(2,1)}, u32[]{:S(2)}) copy-start(bf16[4096,128]{1,0:T(8,128)(2,1)} %param.19) | copy-start | bytes 3145732
  41.7 4.3 %collective-permute-start = (bf16[128,256]{0,1:T(8,128)(2,1)S(1)}, bf16[128,256]{0,1:T(8,128)(2,1)S(1)}, u32[]{:S(2)}, u32[]{:S(2)}) collective-permute-start(bf16[128,256]{0,1:T(8,128)(2,1)S(1)} %get-tuple-element.233), channel_id=1, source_target_pairs={{0,4},{4,0},{8,12},{12,8},{16,20},{20,16},{24,28},{28,24},{1,5},{5... | collective-permute-start | bytes 196616 | tf_op jit(solution)/shard_map/ppermute | solution.py:18
  44.7 69.8 %copy-start.21 = (f32[2]{0:T(128)S(1)}, f32[2]{0:T(128)}, u32[]{:S(2)}) copy-start(f32[2]{0:T(128)} %param.21) | copy-start | bytes 28
  46.0 34.8 %collective-permute-start.1 = (bf16[128,256]{0,1:T(8,128)(2,1)S(1)}, bf16[128,256]{0,1:T(8,128)(2,1)S(1)}, u32[]{:S(2)}, u32[]{:S(2)}) collective-permute-start(bf16[128,256]{0,1:T(8,128)(2,1)S(1)} %collective-permute-done), channel_id=1, source_target_pairs={{0,8},{8,0},{4,12},{12,4},{16,24},{24,16},{20,28},{28,20},{1,9},{9... | collective-permute-start | bytes 196616 | tf_op jit(solution)/shard_map/ppermute | solution.py:18
  80.9 33.5 %collective-permute-start.2 = (bf16[128,256]{0,1:T(8,128)(2,1)S(1)}, bf16[128,256]{0,1:T(8,128)(2,1)S(1)}, u32[]{:S(2)}, u32[]{:S(2)}) collective-permute-start(bf16[128,256]{0,1:T(8,128)(2,1)S(1)} %collective-permute-done.1), channel_id=1, source_target_pairs={{0,16},{16,0},{4,20},{20,4},{8,24},{24,8},{12,28},{28,12},{1,17},{... | collective-permute-start | bytes 196616 | tf_op jit(solution)/shard_map/ppermute | solution.py:18
  114.5 2.1 %copy-start.12 = (bf16[2048,128]{1,0:T(8,128)(2,1)}, bf16[2048,128]{1,0:T(8,128)(2,1)S(1)}, u32[]{:S(2)}) copy-start(bf16[2048,128]{1,0:T(8,128)(2,1)S(1)} %get-tuple-element.417) | copy-start | bytes 1572868 | tf_op jit(solution)/shard_map/while
  114.5 2.1 %copy-start.18 = (bf16[128,1,2,128]{3,0,2,1:T(8,128)(2,1)}, bf16[128,1,2,128]{3,0,2,1:T(8,128)(2,1)S(1)}, u32[]{:S(2)}) copy-start(bf16[128,1,2,128]{3,0,2,1:T(8,128)(2,1)S(1)} %get-tuple-element.418) | copy-start | bytes 196612 | tf_op jit(solution)/shard_map/while
  119.2 1.2 copy-start.2
  119.6 2.3 %copy-start.4 = (bf16[2048,128]{0,1:T(8,128)(2,1)S(1)}, bf16[2048,128]{0,1:T(8,128)(2,1)}, u32[]{:S(2)}) copy-start(bf16[2048,128]{0,1:T(8,128)(2,1)} %get-tuple-element.416) | copy-start | bytes 1572868 | tf_op jit(solution)/shard_map/while
  120.4 1.7 copy-start.13
  120.4 1.8 copy-start.19
  122.2 2.1 %copy-start.12 = (bf16[2048,128]{1,0:T(8,128)(2,1)}, bf16[2048,128]{1,0:T(8,128)(2,1)S(1)}, u32[]{:S(2)}) copy-start(bf16[2048,128]{1,0:T(8,128)(2,1)S(1)} %get-tuple-element.417) | copy-start | bytes 1572868 | tf_op jit(solution)/shard_map/while
  122.2 2.1 %copy-start.18 = (bf16[128,1,2,128]{3,0,2,1:T(8,128)(2,1)}, bf16[128,1,2,128]{3,0,2,1:T(8,128)(2,1)S(1)}, u32[]{:S(2)}) copy-start(bf16[128,1,2,128]{3,0,2,1:T(8,128)(2,1)S(1)} %get-tuple-element.418) | copy-start | bytes 196612 | tf_op jit(solution)/shard_map/while
  126.9 1.2 copy-start.2
  127.3 2.3 %copy-start.4 = (bf16[2048,128]{0,1:T(8,128)(2,1)S(1)}, bf16[2048,128]{0,1:T(8,128)(2,1)}, u32[]{:S(2)}) copy-start(bf16[2048,128]{0,1:T(8,128)(2,1)} %get-tuple-element.416) | copy-start | bytes 1572868 | tf_op jit(solution)/shard_map/while
  128.1 1.7 copy-start.13
  128.1 1.8 copy-start.19
  129.9 7.1 %collective-permute-start.3 = (bf16[128,256]{0,1:T(8,128)(2,1)S(1)}, bf16[128,256]{0,1:T(8,128)(2,1)}, u32[]{:S(2)}, u32[]{:S(2)}) collective-permute-start(bf16[128,256]{0,1:T(8,128)(2,1)S(1)} %bitcast.182), channel_id=1, source_target_pairs={{0,4},{4,0},{8,12},{12,8},{16,20},{20,16},{24,28},{28,24},{1,5},{5... | collective-permute-start | bytes 196616 | tf_op jit(solution)/shard_map/ppermute | solution.py:18
  133.0 4.2 %copy-start.11 = (bf16[256,256]{1,0:T(8,128)(2,1)}, bf16[256,256]{1,0:T(8,128)(2,1)S(1)}, u32[]{:S(2)}) copy-start(bf16[256,256]{1,0:T(8,128)(2,1)S(1)} %fusion.58) | copy-start | bytes 393220
  133.1 14.1 %collective-permute-start.6 = (bf16[2,256]{1,0:T(2,128)(2,1)S(1)}, bf16[2,256]{1,0:T(2,128)(2,1)S(1)}, u32[]{:S(2)}, u32[]{:S(2)}) collective-permute-start(bf16[2,256]{1,0:T(2,128)(2,1)S(1)} %slice.54), channel_id=1, source_target_pairs={{0,4},{4,8},{8,12},{12,16},{16,20},{20,24},{24,28},{1,5},{5,9},{9,... | collective-permute-start | bytes 3080 | tf_op jit(solution)/shard_map/ppermute | solution.py:24
  137.0 8.0 %collective-permute-start.4 = (bf16[128,256]{0,1:T(8,128)(2,1)}, bf16[128,256]{0,1:T(8,128)(2,1)}, u32[]{:S(2)}, u32[]{:S(2)}) collective-permute-start(bf16[128,256]{0,1:T(8,128)(2,1)} %collective-permute-done.3), channel_id=1, source_target_pairs={{0,8},{8,0},{4,12},{12,4},{16,24},{24,16},{20,28},{28,20},{1,9},{9... | collective-permute-start | bytes 196616 | tf_op jit(solution)/shard_map/ppermute | solution.py:18
  137.3 2.1 %copy-start.14 = (bf16[2048,128]{1,0:T(8,128)(2,1)}, bf16[2048,128]{1,0:T(8,128)(2,1)S(1)}, u32[]{:S(2)}) copy-start(bf16[2048,128]{1,0:T(8,128)(2,1)S(1)} %get-tuple-element.462) | copy-start | bytes 1572868 | tf_op jit(solution)/shard_map/while
  137.4 2.1 %copy-start.16 = (bf16[128,1,2,128]{3,0,2,1:T(8,128)(2,1)}, bf16[128,1,2,128]{3,0,2,1:T(8,128)(2,1)S(1)}, u32[]{:S(2)}) copy-start(bf16[128,1,2,128]{3,0,2,1:T(8,128)(2,1)S(1)} %get-tuple-element.463) | copy-start | bytes 196612 | tf_op jit(solution)/shard_map/while
  142.0 1.2 copy-start.3
  142.5 2.3 %copy-start.5 = (bf16[2048,128]{0,1:T(8,128)(2,1)S(1)}, bf16[2048,128]{0,1:T(8,128)(2,1)}, u32[]{:S(2)}) copy-start(bf16[2048,128]{0,1:T(8,128)(2,1)} %get-tuple-element.461) | copy-start | bytes 1572868 | tf_op jit(solution)/shard_map/while
  143.2 1.7 copy-start.15
  143.2 1.8 copy-start.17
  145.0 8.8 %collective-permute-start.5 = (bf16[128,256]{0,1:T(8,128)(2,1)}, bf16[128,256]{0,1:T(8,128)(2,1)S(1)}, u32[]{:S(2)}, u32[]{:S(2)}) collective-permute-start(bf16[128,256]{0,1:T(8,128)(2,1)} %collective-permute-done.4), channel_id=1, source_target_pairs={{0,16},{16,0},{4,20},{20,4},{8,24},{24,8},{12,28},{28,12},{1,17},{... | collective-permute-start | bytes 196616 | tf_op jit(solution)/shard_map/ppermute | solution.py:18
  158.9 3.6 %collective-permute-start.7 = (bf16[128,2]{0,1:T(2,128)(2,1)S(1)}, bf16[128,2]{0,1:T(2,128)(2,1)S(1)}, u32[]{:S(2)}, u32[]{:S(2)}) collective-permute-start(bf16[128,2]{0,1:T(2,128)(2,1)S(1)} %convert_bitcast_fusion), channel_id=1, source_target_pairs={{0,4},{4,0},{8,12},{12,8},{16,20},{20,16},{24,28},{28,24},{1,5},{5... | collective-permute-start | bytes 1544 | tf_op jit(solution)/shard_map/ppermute | solution.py:18
  162.5 3.6 %collective-permute-start.8 = (bf16[128,2]{0,1:T(2,128)(2,1)S(1)}, bf16[128,2]{0,1:T(2,128)(2,1)S(1)}, u32[]{:S(2)}, u32[]{:S(2)}) collective-permute-start(bf16[128,2]{0,1:T(2,128)(2,1)S(1)} %collective-permute-done.7), channel_id=1, source_target_pairs={{0,8},{8,0},{4,12},{12,4},{16,24},{24,16},{20,28},{28,20},{1,9},{9... | collective-permute-start | bytes 1544 | tf_op jit(solution)/shard_map/ppermute | solution.py:18
  166.1 4.5 %collective-permute-start.9 = (bf16[128,2]{0,1:T(2,128)(2,1)S(1)}, bf16[128,2]{0,1:T(2,128)(2,1)S(1)}, u32[]{:S(2)}, u32[]{:S(2)}) collective-permute-start(bf16[128,2]{0,1:T(2,128)(2,1)S(1)} %collective-permute-done.8), channel_id=1, source_target_pairs={{0,16},{16,0},{4,20},{20,4},{8,24},{24,8},{12,28},{28,12},{1,17},{... | collective-permute-start | bytes 1544 | tf_op jit(solution)/shard_map/ppermute | solution.py:18
Sparse Core Ops, SparseCore 0:
  9.6 25.2 all-gather.3
  37.0 56.6 all-gather.7
  95.9 49.0 all-gather.5
  159.0 29.8 reduce-scatter.1
where the time goes:
time: 196 us; the launch traced here: 195 us
  blocking collectives  65.8 us (34%)
  waiting for transfers between devices  47 us (24%)
  matrix products  24.6 us (13%)
  between operations  19.2 us (10%)
  other arithmetic  17.5 us (9%)
  starting transfers between devices  12.7 us (6%)
  local copies, waits for them, and re-layouts  7.99 us (4%)
    all_gather x1, blocking collectives, local(): lax.all_gather(values, 'sp', axis=0, tiled=True)  33.3 us
    all_gather x1, blocking collectives, local(): lax.all_gather(keys, 'sp', axis=0, tiled=True)  32.5 us
    all_gather x1, waiting for transfers between devices, local(): projected = project(lax.all_gather(tokens, 'tp', axis=0, tiled=True))  18.2 us
    reduce_scatter x1, waiting for transfers between devices, local(): lax.psum_scatter(rounded.astype(jnp.bfloat16), 'tp', scatter_dimension=0,...  17.7 us
    ppermute x9, waiting for transfers between devices, swapped(): return lax.ppermute(block, axis, route)  9.08 us
    ppermute x9, starting transfers between devices, swapped(): return lax.ppermute(block, axis, route)  8.63 us
    another operation x7, other arithmetic  7.65 us
    dot_general x5, matrix products, project(): jnp.dot(normed, weight, preferred_element_type=jnp.float32)  6.7 us
  transfers between devices with their start and end apart: 14, of which 6 were waited for; matrix products, arithmetic and copies ran while one was open for 21% of the time, Pallas kernels for 0%

commit v1 on v0

--- a/solution.py
+++ b/solution.py
@@ -131,7 +131,9 @@
     products = (gate_c.astype(jnp.float32) * inputs_u.astype(jnp.float32)).astype(jnp.bfloat16)
     previous = shifted(products[tok_count - (CONV_K - 1) :], "sp", 1)
     key_whole, value_whole = (
-        lax.all_gather(keys, "sp", axis=0, tiled=True),
+        jnp.concatenate(
+            lax.all_to_all(jnp.stack([keys] * lax.axis_size("sp")), "sp", 0, 0), axis=0
+        ),
         lax.all_gather(values, "sp", axis=0, tiled=True),
     )
     local_heads = queries.shape[1] // HEAD_DIM

time: 196 us -> 193 us (0.985)
  blocking collectives: 65.8 us -> 33.2 us
  waiting for transfers between devices: 47 us -> 65.8 us
  starting transfers between devices: 12.7 us -> 22.3 us
  matrix products: 24.6 us -> 26.8 us
    all_gather x1 -> x0, blocking collectives: 32.5 us -> none  [local(): lax.all_gather(keys, 'sp', axis=0, tiled=True)]
    all_gather x2, waiting for transfers between devices: 0.01 us -> 10.8 us  [local(): pieces = lax.all_gather((w_out_att, w_out_conv), 'sp', axis=0, tiled=True)]
    ppermute x9, waiting for transfers between devices: 9.08 us -> 15.9 us  [swapped(): return lax.ppermute(block, axis, route)]
    all_to_all x0 -> x1, starting transfers between devices: none -> 5.52 us  [local(): lax.all_to_all(jnp.stack([keys] * lax.axis_size('sp')), 'sp', 0, 0)]
    ppermute x9, starting transfers between devices: 8.63 us -> 12.6 us  [swapped(): return lax.ppermute(block, axis, route)]
    dot_general x5, matrix products: 6.7 us -> 9.07 us  [project(): jnp.dot(normed, weight, preferred_element_type=jnp.float32)]
  transfers between devices with their start and end apart: 14 -> 15, of which waited for: 6 -> 9; matrix products, arithmetic and copies ran while one was open for 21% -> 23% of each run, Pallas kernels for 0% -> 0%
where the time goes in v1:
time: 193 us
  waiting for transfers between devices  65.8 us (34%)
  blocking collectives  33.2 us (17%)
  matrix products  26.8 us (14%)
  starting transfers between devices  22.3 us (12%)
  between operations  18.9 us (10%)
  other arithmetic  17.5 us (9%)
  local copies, waits for them, and re-layouts  8.05 us (4%)
    all_gather x1, blocking collectives, local(): lax.all_gather(values, 'sp', axis=0, tiled=True)  33.2 us
    all_gather x1, waiting for transfers between devices, local(): projected = project(lax.all_gather(tokens, 'tp', axis=0, tiled=True))  19.1 us
    reduce_scatter x1, waiting for transfers between devices, local(): lax.psum_scatter(rounded.astype(jnp.bfloat16), 'tp', scatter_dimension=0,...  17.6 us
    ppermute x9, waiting for transfers between devices, swapped(): return lax.ppermute(block, axis, route)  15.9 us
    ppermute x9, starting transfers between devices, swapped(): return lax.ppermute(block, axis, route)  12.6 us
    all_gather x2, waiting for transfers between devices, local(): pieces = lax.all_gather((w_out_att, w_out_conv), 'sp', axis=0, tiled=True)  10.8 us
    dot_general x5, matrix products, project(): jnp.dot(normed, weight, preferred_element_type=jnp.float32)  9.07 us
    another operation x7, other arithmetic  7.65 us
  transfers between devices with their start and end apart: 15, of which 9 were waited for; matrix products, arithmetic and copies ran while one was open for 23% of the time, Pallas kernels for 0%

profile of v1, /device:TPU:0, one launch (start us, length us, event | category | flops | bytes accessed | tf_op | source)
XLA Modules:
  0.0 193.0 jit_solution(14824080870777596703)
XLA Ops:
  7.2 0.7 all-gather.4.cloned.1.call-update
  8.0 0.7 all-gather.8.cloned.1.call-update
  8.7 0.7 all-gather.6.cloned.1.call-update
  9.4 0.6 add_reduce_fusion
  12.0 0.6 add_reduce_fusion.1
  15.0 0.8 fusion.88
  15.8 19.1 %all-gather.4.cloned.1.call-done = bf16[256,4096]{1,0:T(8,128)(2,1)} async-done(((bf16[64,4096]{1,0:T(8,128)(2,1)}), bf16[256,4096]{1,0:T(8,128)(2,1)}) %all-gather.4.cloned.1.call-update) | async-done | bytes 2097168 | tf_op jit(solution)/shard_map/all_gather | solution.py:121
  34.9 2.2 %fusion.53 = f32[256]{0:T(256)S(1)} fusion(bf16[256,4096]{1,0:T(8,128)(2,1)} %all-gather.4.cloned.1.call-done), kind=kLoop, calls=%fused_computation.78 | loop fusion | flops 3145472 | bytes 2098176 | tf_op jit(solution)/shard_map/reduce_sum | solution.py:29
  37.1 0.6 fusion.55
  37.8 1.4 copy-done.1
  39.2 0.7 convolution_convert_fusion.4
  39.9 0.9 stack.2
  40.8 5.5 %all-to-all-start = ((bf16[8,256,128]{2,1,0:T(8,128)(2,1)}), bf16[8,256,128]{2,1,0:T(8,128)(2,1)S(1)}, u32[]{:S(2)}, u32[]{:S(2)}) async-start(bf16[8,256,128]{2,1,0:T(8,128)(2,1)} %stack.2), calls=%async_computation | async-start | bytes 1048576 | tf_op jit(solution)/shard_map/all_to_all | solution.py:135
  46.3 3.3 %convolution_convert_fusion.3 = bf16[256,256]{0,1:T(8,128)(2,1)S(1)} fusion(bf16[256,4096]{1,0:T(8,128)(2,1)} %copy-done.1, bf16[4096,256]{1,0:T(8,128)(2,1)} %param.18), kind=kOutput, calls=%fused_computation.91 | convolution fusion | flops 536936448 | bytes 4325376 | tf_op jit(solution)/shard_map/dot_general | solution.py:115
  49.7 2.0 %collective-permute-start = (bf16[128,256]{0,1:T(8,128)(2,1)S(1)}, bf16[128,256]{0,1:T(8,128)(2,1)S(1)}, u32[]{:S(2)}, u32[]{:S(2)}) collective-permute-start(bf16[128,256]{0,1:T(8,128)(2,1)S(1)} %get-tuple-element.233), channel_id=1, source_target_pairs={{0,4},{4,0},{8,12},{12,8},{16,20},{20,16},{24,28},{28,24},{1,5},{5... | collective-permute-start | bytes 196616 | tf_op jit(solution)/shard_map/ppermute | solution.py:18
  51.7 1.4 fusion.59
  53.1 1.2 collective-permute-done
  54.4 1.8 collective-permute-start.1
  56.2 0.7 convolution_convert_fusion.5
  56.9 7.0 %collective-permute-done.1 = bf16[128,256]{0,1:T(8,128)(2,1)S(1)} collective-permute-done((bf16[128,256]{0,1:T(8,128)(2,1)S(1)}, bf16[128,256]{0,1:T(8,128)(2,1)S(1)}, u32[]{:S(2)}, u32[]{:S(2)}) %collective-permute-start.1) | collective-permute-done | bytes 65568 | tf_op jit(solution)/shard_map/ppermute | solution.py:18
  63.9 4.6 %collective-permute-start.2 = (bf16[128,256]{0,1:T(8,128)(2,1)S(1)}, bf16[128,256]{0,1:T(8,128)(2,1)S(1)}, u32[]{:S(2)}, u32[]{:S(2)}) collective-permute-start(bf16[128,256]{0,1:T(8,128)(2,1)S(1)} %collective-permute-done.1), channel_id=1, source_target_pairs={{0,16},{16,0},{4,20},{20,4},{8,24},{24,8},{12,28},{28,12},{1,17},{... | collective-permute-start | bytes 196616 | tf_op jit(solution)/shard_map/ppermute | solution.py:18
  68.5 33.2 %all_gather.13 = bf16[2048,128]{1,0:T(8,128)(2,1)S(1)} all-gather(bf16[256,128]{1,0:T(8,128)(2,1)S(1)} %convolution_convert_fusion.5), channel_id=1, replica_groups=mesh['sp'=8,'tp'=4] {'sp'}, dimensions={0}, use_global_device_ids=true | all-gather | bytes 589824 | tf_op jit(solution)/shard_map/all_gather | solution.py:137
  101.7 1.0 copy.20
  102.9 15.4 %while.27 = (s32[]{:T(128)}, f32[128,1,2,128]{0,3,2,1:T(8,128)S(1)}, f32[128,1,2]{0,2,1:T(2,128)S(1)}, s32[]{:T(128)}, s32[]{:T(128)}, /*index=5*/bf16[2048,128]...) while((s32[]{:T(128)}, ...), condition=%wide.region_12.13_spmd.clone, body=%wide.region_8.12_spmd.clone.sunk | while | flops 175588480 | bytes 23864196 | solution.py:73
  103.1 1.8 fusion.127
  105.0 2.5 %fusion.128 = f32[128,1,2,8,128]{0,3,2,1,4:T(8,128)S(1)} fusion(f32[128,1,2,8,128]{0,4,3,2,1:T(8,128)S(1)} %bitcast.179), kind=kOutput, calls=%fused_computation.56.clone.1 | output fusion | flops 33292288 | bytes 2097152 | tf_op jit(solution)/shard_map/reduce-window.2
  108.0 0.8 copy-done.3
  108.8 1.5 fusion.129
  110.8 1.8 fusion.127
  112.7 2.5 %fusion.128 = f32[128,1,2,8,128]{0,3,2,1,4:T(8,128)S(1)} fusion(f32[128,1,2,8,128]{0,4,3,2,1:T(8,128)S(1)} %bitcast.179), kind=kOutput, calls=%fused_computation.56.clone.1 | output fusion | flops 33292288 | bytes 2097152 | tf_op jit(solution)/shard_map/reduce-window.2
  115.7 0.8 copy-done.3
  116.5 1.5 fusion.129
  118.3 3.0 %fusion.58 = bf16[256,256]{1,0:T(8,128)(2,1)S(1)} fusion(f32[256,256]{1,0:T(8,128)} %fusion.59, bf16[256,4096]{1,0:T(8,128)(2,1)} %copy-done.1, bf16[4096,256]{1,0:T(8,128)(2,1)} %param.24), kind=kOutput, calls=%fused_computation.84 | convolution fusion | flops 537133056 | bytes 4587520 | tf_op jit(solution)/shard_map/dot_general | solution.py:115
  121.3 4.1 %collective-permute-start.6 = (bf16[2,256]{1,0:T(2,128)(2,1)S(1)}, bf16[2,256]{1,0:T(2,128)(2,1)S(1)}, u32[]{:S(2)}, u32[]{:S(2)}) collective-permute-start(bf16[2,256]{1,0:T(2,128)(2,1)S(1)} %slice.54), channel_id=1, source_target_pairs={{0,4},{4,8},{8,12},{12,16},{16,20},{20,24},{24,28},{1,5},{5,9},{9,... | collective-permute-start | bytes 3080 | tf_op jit(solution)/shard_map/ppermute | solution.py:24
  126.5 6.5 %fusion.63 = f32[256,4096]{1,0:T(8,128)} fusion(bf16[4096,256]{1,0:T(8,128)(2,1)} %all-gather.8.cloned.1.call-done, bf16[256,4096]{1,0:T(8,128)(2,1)} %copy-done.1, bf16[4096,256]{1,0:T(8,128)(2,1)S(1)} %copy-done, bf16[256,256]{1,0:T(8,128)(2,1)S(1)} %fusion.58, bf16[2,256]{1,0:T(2,128)(2,1)S(1)} %collective-permute-done.6, f32[256]{0:T(256)S(1)} %bitcast.188, ...), kind=kOutput, calls=%fused_computation.92 | convolution fusion | flops 1074921472 | bytes 10620928 | tf_op jit(solution)/shard_map/dot_general | solution.py:169
  133.1 7.7 %while.26 = (s32[]{:T(128)}, f32[128,1,2,128]{0,3,2,1:T(8,128)S(1)}, f32[128,1,2]{0,2,1:T(2,128)S(1)}, s32[]{:T(128)}, s32[]{:T(128)}, /*index=5*/bf16[2048,128]...) while((s32[]{:T(128)}, ...), condition=%wide.region_6.7_spmd.clone, body=%wide.region_2.6_spmd.clone.sunk | while | flops 175588480 | bytes 23864196 | solution.py:73
  133.4 1.8 fusion.120
  135.2 2.5 %fusion.121 = f32[128,1,2,8,128]{0,3,2,1,4:T(8,128)S(1)} fusion(f32[128,1,2,8,128]{0,4,3,2,1:T(8,128)S(1)} %bitcast.180), kind=kOutput, calls=%fused_computation.20.clone.1 | output fusion | flops 33292288 | bytes 2097152 | tf_op jit(solution)/shard_map/reduce-window
  138.2 0.8 copy-done.4
  139.0 1.5 fusion.122
  140.8 10.8 %all-gather.6.cloned.1.call-done = bf16[4096,256]{1,0:T(8,128)(2,1)} async-done(((bf16[512,256]{1,0:T(8,128)(2,1)}), bf16[4096,256]{1,0:T(8,128)(2,1)}) %all-gather.6.cloned.1.call-update) | async-done | bytes 2097168 | tf_op jit(solution)/shard_map/all_gather | solution.py:167
  151.6 5.0 %fusion.52 = bf16[256,4096]{1,0:T(8,128)(2,1)} fusion(f32[256,4096]{1,0:T(8,128)} %fusion.63, bf16[4096,256]{1,0:T(8,128)(2,1)} %all-gather.6.cloned.1.call-done, bf16[128,256]{0,1:T(8,128)(2,1)S(1)} %collective-permute-done.5, bf16[128,256]{0,1:T(8,128)(2,1)S(1)} %bitcast.182), kind=kOutput, calls=%fused_computation.77 | convolution fusion | flops 539230208 | bytes 8519680 | tf_op jit(solution)/shard_map/dot_general | solution.py:168
  157.3 3.0 %collective-permute-done.7 = bf16[128,2]{0,1:T(2,128)(2,1)S(1)} collective-permute-done((bf16[128,2]{0,1:T(2,128)(2,1)S(1)}, bf16[128,2]{0,1:T(2,128)(2,1)S(1)}, u32[]{:S(2)}, u32[]{:S(2)}) %collective-permute-start.7) | collective-permute-done | bytes 544 | tf_op jit(solution)/shard_map/ppermute | solution.py:18
  160.3 1.5 collective-permute-start.8
  161.8 2.0 %collective-permute-done.8 = bf16[128,2]{0,1:T(2,128)(2,1)S(1)} collective-permute-done((bf16[128,2]{0,1:T(2,128)(2,1)S(1)}, bf16[128,2]{0,1:T(2,128)(2,1)S(1)}, u32[]{:S(2)}, u32[]{:S(2)}) %collective-permute-start.8) | collective-permute-done | bytes 544 | tf_op jit(solution)/shard_map/ppermute | solution.py:18
  163.9 1.9 collective-permute-start.9
  165.7 2.6 %collective-permute-done.9 = bf16[128,2]{0,1:T(2,128)(2,1)S(1)} collective-permute-done((bf16[128,2]{0,1:T(2,128)(2,1)S(1)}, bf16[128,2]{0,1:T(2,128)(2,1)S(1)}, u32[]{:S(2)}, u32[]{:S(2)}) %collective-permute-start.9) | collective-permute-done | bytes 544 | tf_op jit(solution)/shard_map/ppermute | solution.py:18
  168.9 17.6 %reduce-scatter.2.cloned.1.call-done = bf16[64,4096]{1,0:T(8,128)(2,1)} async-done(((bf16[256,4096]{1,0:T(8,128)(2,1)}), bf16[64,4096]{1,0:T(8,128)(2,1)}) %reduce-scatter.2.cloned.1.call-update) | async-done | bytes 524304 | tf_op jit(solution)/shard_map/reduce_scatter | solution.py:173
  (110 shorter events, 5.0 us)
Async XLA Ops:
  7.2 119.4 %copy-start = (bf16[4096,256]{1,0:T(8,128)(2,1)S(1)}, bf16[4096,256]{1,0:T(8,128)(2,1)}, u32[]{:S(2)}) copy-start(bf16[4096,256]{1,0:T(8,128)(2,1)} %param.22) | copy-start | bytes 6291460
  7.2 29.9 %copy-start.19 = (f32[4096]{0:T(1024)S(1)}, f32[4096]{0:T(1024)}, u32[]{:S(2)}) copy-start(f32[4096]{0:T(1024)} %param.17) | copy-start | bytes 49156
  7.2 27.7 %all-gather.4.cloned.1.call-start = ((), (), s32[]{:S(2)}) async-start(), calls=%async_computation.2 | async-start | bytes 2621440 | tf_op jit(solution)/shard_map/all_gather | solution.py:121
  7.9 118.6 %all-gather.8.cloned.1.call-start = ((), (), s32[]{:S(2)}) async-start(), calls=%async_computation.4 | async-start | bytes 2359296 | tf_op jit(solution)/shard_map/all_gather | solution.py:167
  8.7 143.0 %all-gather.6.cloned.1.call-start = ((), (), s32[]{:S(2)}) async-start(), calls=%async_computation.3 | async-start | bytes 2359296 | tf_op jit(solution)/shard_map/all_gather | solution.py:167
  34.9 2.3 %copy-start.7 = (bf16[256,4096]{1,0:T(8,128)(2,1)S(1)}, bf16[256,4096]{1,0:T(8,128)(2,1)}, u32[]{:S(2)}) copy-start(bf16[256,4096]{1,0:T(8,128)(2,1)} %all-gather.4.cloned.1.call-done) | copy-start | bytes 6291460
  37.1 2.1 %copy-start.9 = (bf16[4096,128]{1,0:T(8,128)(2,1)S(1)}, bf16[4096,128]{1,0:T(8,128)(2,1)}, u32[]{:S(2)}) copy-start(bf16[4096,128]{1,0:T(8,128)(2,1)} %param.19) | copy-start | bytes 3145732
  37.8 1.4 copy-start.1
  40.8 62.1 %all-to-all-start = ((bf16[8,256,128]{2,1,0:T(8,128)(2,1)}), bf16[8,256,128]{2,1,0:T(8,128)(2,1)S(1)}, u32[]{:S(2)}, u32[]{:S(2)}) async-start(bf16[8,256,128]{2,1,0:T(8,128)(2,1)} %stack.2), calls=%async_computation | async-start | bytes 1048576 | tf_op jit(solution)/shard_map/all_to_all | solution.py:135
  46.3 140.2 %reduce-scatter.2.cloned.1.call-start = ((), (), s32[]{:S(2)}) async-start(), calls=%async_computation.5 | async-start | bytes 2621440 | tf_op jit(solution)/shard_map/reduce_scatter | solution.py:173
  46.3 5.4 %copy-start.2 = (bf16[256,4096]{1,0:T(8,128)(2,1)S(1)}, bf16[256,4096]{1,0:T(8,128)(2,1)}, u32[]{:S(2)}) copy-start(bf16[256,4096]{1,0:T(8,128)(2,1)} %copy-done.1) | copy-start | bytes 6291460
  46.3 5.4 %copy-start.8 = (bf16[4096,256]{1,0:T(8,128)(2,1)S(1)}, bf16[4096,256]{1,0:T(8,128)(2,1)}, u32[]{:S(2)}) copy-start(bf16[4096,256]{1,0:T(8,128)(2,1)} %param.23) | copy-start | bytes 6291460
  49.7 6.5 %copy-start.10 = (bf16[4096,128]{1,0:T(8,128)(2,1)S(1)}, bf16[4096,128]{1,0:T(8,128)(2,1)}, u32[]{:S(2)}) copy-start(bf16[4096,128]{1,0:T(8,128)(2,1)} %param.20) | copy-start | bytes 3145732
  49.7 4.7 %collective-permute-start = (bf16[128,256]{0,1:T(8,128)(2,1)S(1)}, bf16[128,256]{0,1:T(8,128)(2,1)S(1)}, u32[]{:S(2)}, u32[]{:S(2)}) collective-permute-start(bf16[128,256]{0,1:T(8,128)(2,1)S(1)} %get-tuple-element.233), channel_id=1, source_target_pairs={{0,4},{4,0},{8,12},{12,8},{16,20},{20,16},{24,28},{28,24},{1,5},{5... | collective-permute-start | bytes 196616 | tf_op jit(solution)/shard_map/ppermute | solution.py:18
  53.1 49.7 %copy-start.20 = (f32[2]{0:T(128)S(1)}, f32[2]{0:T(128)}, u32[]{:S(2)}) copy-start(f32[2]{0:T(128)} %param.21) | copy-start | bytes 28
  54.4 9.6 %collective-permute-start.1 = (bf16[128,256]{0,1:T(8,128)(2,1)S(1)}, bf16[128,256]{0,1:T(8,128)(2,1)S(1)}, u32[]{:S(2)}, u32[]{:S(2)}) collective-permute-start(bf16[128,256]{0,1:T(8,128)(2,1)S(1)} %collective-permute-done), channel_id=1, source_target_pairs={{0,8},{8,0},{4,12},{12,4},{16,24},{24,16},{20,28},{28,20},{1,9},{9... | collective-permute-start | bytes 196616 | tf_op jit(solution)/shard_map/ppermute | solution.py:18
  63.9 38.8 %collective-permute-start.2 = (bf16[128,256]{0,1:T(8,128)(2,1)S(1)}, bf16[128,256]{0,1:T(8,128)(2,1)S(1)}, u32[]{:S(2)}, u32[]{:S(2)}) collective-permute-start(bf16[128,256]{0,1:T(8,128)(2,1)S(1)} %collective-permute-done.1), channel_id=1, source_target_pairs={{0,16},{16,0},{4,20},{20,4},{8,24},{24,8},{12,28},{28,12},{1,17},{... | collective-permute-start | bytes 196616 | tf_op jit(solution)/shard_map/ppermute | solution.py:18
  102.9 2.1 %copy-start.11 = (bf16[2048,128]{1,0:T(8,128)(2,1)}, bf16[2048,128]{1,0:T(8,128)(2,1)S(1)}, u32[]{:S(2)}) copy-start(bf16[2048,128]{1,0:T(8,128)(2,1)S(1)} %get-tuple-element.417) | copy-start | bytes 1572868 | tf_op jit(solution)/shard_map/while
  102.9 2.1 %copy-start.17 = (bf16[128,1,2,128]{3,0,2,1:T(8,128)(2,1)}, bf16[128,1,2,128]{3,0,2,1:T(8,128)(2,1)S(1)}, u32[]{:S(2)}) copy-start(bf16[128,1,2,128]{3,0,2,1:T(8,128)(2,1)S(1)} %get-tuple-element.418) | copy-start | bytes 196612 | tf_op jit(solution)/shard_map/while
  107.5 1.2 copy-start.3
  108.0 2.3 %copy-start.5 = (bf16[2048,128]{0,1:T(8,128)(2,1)S(1)}, bf16[2048,128]{0,1:T(8,128)(2,1)}, u32[]{:S(2)}) copy-start(bf16[2048,128]{0,1:T(8,128)(2,1)} %get-tuple-element.416) | copy-start | bytes 1572868 | tf_op jit(solution)/shard_map/while
  108.8 1.7 copy-start.12
  108.8 1.8 copy-start.18
  110.6 2.1 %copy-start.11 = (bf16[2048,128]{1,0:T(8,128)(2,1)}, bf16[2048,128]{1,0:T(8,128)(2,1)S(1)}, u32[]{:S(2)}) copy-start(bf16[2048,128]{1,0:T(8,128)(2,1)S(1)} %get-tuple-element.417) | copy-start | bytes 1572868 | tf_op jit(solution)/shard_map/while
  110.6 2.1 %copy-start.17 = (bf16[128,1,2,128]{3,0,2,1:T(8,128)(2,1)}, bf16[128,1,2,128]{3,0,2,1:T(8,128)(2,1)S(1)}, u32[]{:S(2)}) copy-start(bf16[128,1,2,128]{3,0,2,1:T(8,128)(2,1)S(1)} %get-tuple-element.418) | copy-start | bytes 196612 | tf_op jit(solution)/shard_map/while
  115.2 1.2 copy-start.3
  115.7 2.3 %copy-start.5 = (bf16[2048,128]{0,1:T(8,128)(2,1)S(1)}, bf16[2048,128]{0,1:T(8,128)(2,1)}, u32[]{:S(2)}) copy-start(bf16[2048,128]{0,1:T(8,128)(2,1)} %get-tuple-element.416) | copy-start | bytes 1572868 | tf_op jit(solution)/shard_map/while
  116.5 1.7 copy-start.12
  116.5 1.8 copy-start.18
  118.3 7.9 %collective-permute-start.3 = (bf16[128,256]{0,1:T(8,128)(2,1)S(1)}, bf16[128,256]{0,1:T(8,128)(2,1)S(1)}, u32[]{:S(2)}, u32[]{:S(2)}) collective-permute-start(bf16[128,256]{0,1:T(8,128)(2,1)S(1)} %bitcast.184), channel_id=1, source_target_pairs={{0,4},{4,0},{8,12},{12,8},{16,20},{20,16},{24,28},{28,24},{1,5},{5... | collective-permute-start | bytes 196616 | tf_op jit(solution)/shard_map/ppermute | solution.py:18
  121.3 5.2 %collective-permute-start.6 = (bf16[2,256]{1,0:T(2,128)(2,1)S(1)}, bf16[2,256]{1,0:T(2,128)(2,1)S(1)}, u32[]{:S(2)}, u32[]{:S(2)}) collective-permute-start(bf16[2,256]{1,0:T(2,128)(2,1)S(1)} %slice.54), channel_id=1, source_target_pairs={{0,4},{4,8},{8,12},{12,16},{16,20},{20,24},{24,28},{1,5},{5,9},{9,... | collective-permute-start | bytes 3080 | tf_op jit(solution)/shard_map/ppermute | solution.py:24
  126.1 6.9 %collective-permute-start.4 = (bf16[128,256]{0,1:T(8,128)(2,1)S(1)}, bf16[128,256]{0,1:T(8,128)(2,1)}, u32[]{:S(2)}, u32[]{:S(2)}) collective-permute-start(bf16[128,256]{0,1:T(8,128)(2,1)S(1)} %collective-permute-done.3), channel_id=1, source_target_pairs={{0,8},{8,0},{4,12},{12,4},{16,24},{24,16},{20,28},{28,20},{1,9},{9... | collective-permute-start | bytes 196616 | tf_op jit(solution)/shard_map/ppermute | solution.py:18
  133.0 18.6 %collective-permute-start.5 = (bf16[128,256]{0,1:T(8,128)(2,1)}, bf16[128,256]{0,1:T(8,128)(2,1)S(1)}, u32[]{:S(2)}, u32[]{:S(2)}) collective-permute-start(bf16[128,256]{0,1:T(8,128)(2,1)} %collective-permute-done.4), channel_id=1, source_target_pairs={{0,16},{16,0},{4,20},{20,4},{8,24},{24,8},{12,28},{28,12},{1,17},{... | collective-permute-start | bytes 196616 | tf_op jit(solution)/shard_map/ppermute | solution.py:18
  133.1 2.1 %copy-start.13 = (bf16[2048,128]{1,0:T(8,128)(2,1)}, bf16[2048,128]{1,0:T(8,128)(2,1)S(1)}, u32[]{:S(2)}) copy-start(bf16[2048,128]{1,0:T(8,128)(2,1)S(1)} %get-tuple-element.462) | copy-start | bytes 1572868 | tf_op jit(solution)/shard_map/while
  133.1 2.1 %copy-start.15 = (bf16[128,1,2,128]{3,0,2,1:T(8,128)(2,1)}, bf16[128,1,2,128]{3,0,2,1:T(8,128)(2,1)S(1)}, u32[]{:S(2)}) copy-start(bf16[128,1,2,128]{3,0,2,1:T(8,128)(2,1)S(1)} %get-tuple-element.463) | copy-start | bytes 196612 | tf_op jit(solution)/shard_map/while
  137.7 1.2 copy-start.4
  138.2 2.3 %copy-start.6 = (bf16[2048,128]{0,1:T(8,128)(2,1)S(1)}, bf16[2048,128]{0,1:T(8,128)(2,1)}, u32[]{:S(2)}) copy-start(bf16[2048,128]{0,1:T(8,128)(2,1)} %get-tuple-element.461) | copy-start | bytes 1572868 | tf_op jit(solution)/shard_map/while
  139.0 1.7 copy-start.14
  139.0 1.8 copy-start.16
  156.6 3.6 %collective-permute-start.7 = (bf16[128,2]{0,1:T(2,128)(2,1)S(1)}, bf16[128,2]{0,1:T(2,128)(2,1)S(1)}, u32[]{:S(2)}, u32[]{:S(2)}) collective-permute-start(bf16[128,2]{0,1:T(2,128)(2,1)S(1)} %convert_bitcast_fusion), channel_id=1, source_target_pairs={{0,4},{4,0},{8,12},{12,8},{16,20},{20,16},{24,28},{28,24},{1,5},{5... | collective-permute-start | bytes 1544 | tf_op jit(solution)/shard_map/ppermute | solution.py:18
  160.3 3.6 %collective-permute-start.8 = (bf16[128,2]{0,1:T(2,128)(2,1)S(1)}, bf16[128,2]{0,1:T(2,128)(2,1)S(1)}, u32[]{:S(2)}, u32[]{:S(2)}) collective-permute-start(bf16[128,2]{0,1:T(2,128)(2,1)S(1)} %collective-permute-done.7), channel_id=1, source_target_pairs={{0,8},{8,0},{4,12},{12,4},{16,24},{24,16},{20,28},{28,20},{1,9},{9... | collective-permute-start | bytes 1544 | tf_op jit(solution)/shard_map/ppermute | solution.py:18
  163.9 4.5 %collective-permute-start.9 = (bf16[128,2]{0,1:T(2,128)(2,1)S(1)}, bf16[128,2]{0,1:T(2,128)(2,1)S(1)}, u32[]{:S(2)}, u32[]{:S(2)}) collective-permute-start(bf16[128,2]{0,1:T(2,128)(2,1)S(1)} %collective-permute-done.8), channel_id=1, source_target_pairs={{0,16},{16,0},{4,20},{20,4},{8,24},{24,8},{12,28},{28,12},{1,17},{... | collective-permute-start | bytes 1544 | tf_op jit(solution)/shard_map/ppermute | solution.py:18
Sparse Core Ops, SparseCore 0:
  9.6 25.2 all-gather.3
  37.0 63.7 all-gather.7
  102.9 48.6 all-gather.5
  156.8 29.6 reduce-scatter.1
